TPU v7x, 32 devices: a whole 2x2x4 slice. The times are simulated.
32 devices in a mesh: fs: 16 (over z, y, core), tp: 2 (over x).
Axes of the slice: x: 2, y: 2, z: 4, core: 2. Of those that a mesh axis runs over, the one named last changes fastest.
Arguments:
- tokens: bfloat16 [6144, 2048], P('fs', 'tp'), may hold values from -60 to 60
- gain_mixer: float32 [2048], P('tp'), may hold values from 0.1 to 1.9
- w_in: bfloat16 [2048, 1024], P('fs', 'tp'), may hold values from -0.125 to 0.125
- pool_scale: float32 [1024], P('tp'), may hold values from 0.1 to 1.9
- w_pool_out: bfloat16 [2048, 1024], P('fs', 'tp'), may hold values from -0.25 to 0.25
- gain_mid: float32 [2048], P('tp'), may hold values from 0.1 to 1.9
- w_ff1: bfloat16 [2048, 8192], P('fs', 'tp'), may hold values from -0.125 to 0.125
- w_ff2: bfloat16 [2048, 8192], P('fs', 'tp'), may hold values from -0.09375 to 0.09375
- gain_out: float32 [2048], P('tp'), may hold values from 0.1 to 1.9
Outputs:
- layer_out: bfloat16 [6144, 2048], P('fs', 'tp')
All inputs are finite; a program needn't handle non-finite values.
Results may differ from a plain program's by a relative error of at most 0.017.
Values may be sent and summed in bfloat16 or wider, within the bound.
A program may use at most 128 MiB of HBM per device.

v0:
```python
import jax
import jax.numpy as jnp
from jax import lax
from jax.sharding import PartitionSpec as P

norm_eps = 1e-05
residual_alpha = 2.0**0.25


def row_norm(value, gain):
    width = value.shape[1] * lax.axis_size("tp")
    total, squares = lax.psum((jnp.sum(value, axis=1), jnp.sum(value * value, axis=1)), "tp")
    mean = (total / width)[:, None]
    spread = (squares / width)[:, None] - mean * mean
    return (value - mean) * lax.rsqrt(spread + norm_eps) * gain


def shifted(value, steps):
    return jnp.pad(value, ((steps, 0), (0, 0)))[: value.shape[0]]


def project_rows(weight, left):
    return lax.dot_general(
        weight, left, (((1,), (1,)), ((), ())), preferred_element_type=jnp.float32
    )


def fold_features(weight, piece):
    return jnp.dot(piece, weight, preferred_element_type=jnp.float32)


def local(tokens, gain_mixer, w_in, pool_scale, w_pool_out, gain_mid, w_ff1, w_ff2, gain_out):
    xf = tokens.astype(jnp.float32)
    length = tokens.shape[0]
    mixed_in = row_norm(xf, gain_mixer).astype(jnp.bfloat16)
    in_full = lax.all_gather(w_in, "fs", axis=0, tiled=True)
    channels = w_in.shape[1]
    pool_in = fold_features(in_full, lax.all_gather(mixed_in, "tp", axis=1, tiled=True))
    uf = pool_in.astype(jnp.bfloat16).astype(jnp.float32)
    group_width = channels * lax.axis_size("tp") // 4
    channel = lax.axis_index("tp") * channels + jnp.arange(channels, dtype=jnp.int32)
    group = channel // group_width
    sum_two = uf + shifted(uf, 1)
    sum_four = sum_two + shifted(sum_two, 2)
    sum_eight = sum_four + shifted(sum_four, 4)
    sum_sixteen = sum_eight + shifted(sum_eight, 8)
    window_sum = jnp.where(
        group == 0,
        sum_two,
        jnp.where(group == 1, sum_four, jnp.where(group == 2, sum_eight, sum_sixteen)),
    )
    window = jnp.where(
        group == 0, 2.0, jnp.where(group == 1, 4.0, jnp.where(group == 2, 8.0, 16.0))
    ).astype(jnp.float32)
    position = jnp.arange(length, dtype=jnp.float32)[:, None]
    count = jnp.minimum(position + 1.0, window[None, :])
    pooled = ((window_sum / count - uf) * pool_scale).astype(jnp.bfloat16)
    out_full = lax.all_gather(w_pool_out, "fs", axis=0, tiled=True)
    mixer_out = lax.psum_scatter(
        project_rows(out_full, pooled).astype(jnp.bfloat16), "tp", scatter_dimension=0, tiled=True
    ).astype(jnp.float32)
    mixer_out = mixer_out.astype(jnp.bfloat16).T
    middle = row_norm(residual_alpha * xf + mixer_out.astype(jnp.float32), gain_mid).astype(
        jnp.bfloat16
    )
    up_full = lax.all_gather(w_ff1, "fs", axis=0, tiled=True)
    upward = fold_features(up_full, lax.all_gather(middle, "tp", axis=1, tiled=True))
    hidden = jnp.square(jax.nn.relu(upward)).astype(jnp.bfloat16)
    down_full = lax.all_gather(w_ff2, "fs", axis=0, tiled=True)
    ff_out = lax.psum_scatter(
        project_rows(down_full, hidden).astype(jnp.bfloat16), "tp", scatter_dimension=0, tiled=True
    ).astype(jnp.float32)
    ff_out = ff_out.astype(jnp.bfloat16).T
    result = row_norm(
        residual_alpha * middle.astype(jnp.float32) + ff_out.astype(jnp.float32), gain_out
    )
    return result.astype(jnp.bfloat16)


def solution(mesh):
    return jax.shard_map(
        local,
        mesh=mesh,
        in_specs=(
            P("fs", "tp"),
            P("tp"),
            P("fs", "tp"),
            P("tp"),
            P("fs", "tp"),
            P("tp"),
            P("fs", "tp"),
            P("fs", "tp"),
            P("tp"),
        ),
        out_specs=P("fs", "tp"),
        check_vma=False,
    )
```

profile of v0, /device:TPU:0, one launch (start us, length us, event | category | flops | bytes accessed | tf_op | source)
XLA Modules:
  0.0 509.2 jit_solution(2410414311106388984)
XLA Ops:
  6.5 1.4 convert_reduce_fusion
  8.0 5.9 %all-reduce.6 = (f32[384]{0:T(512)S(1)}, f32[384]{0:T(512)S(1)}) all-reduce(f32[384]{0:T(512)S(1)} %get-tuple-element.10, f32[384]{0:T(512)S(1)} %get-tuple-element.9), channel_id=1, replica_groups=mesh['fs'=16,'tp'=2] {'tp'}, use_global_device_ids=true, to_apply=%region_3.0 | all-reduce | flops 768 | bytes 6144 | tf_op jit(solution)/shard_map/psum | solution.py:12
  13.9 2.3 fusion.7
  16.3 0.7 all-gather.9.cloned.1.call-update
  17.0 0.7 all-gather.11.cloned.1.call-update
  17.8 27.5 %all-gather.7.cloned.1.call-done = bf16[384,2048]{1,0:T(8,128)(2,1)} async-done(((bf16[384,1024]{1,0:T(8,128)(2,1)}), bf16[384,2048]{1,0:T(8,128)(2,1)}) %all-gather.7.cloned.1.call-update) | async-done | bytes 1572880 | tf_op jit(solution)/shard_map/all_gather | solution.py:38
  45.3 43.7 %all-gather.9.cloned.1.call-done = bf16[2048,512]{1,0:T(8,128)(2,1)} async-done(((bf16[128,512]{1,0:T(8,128)(2,1)}), bf16[2048,512]{1,0:T(8,128)(2,1)}) %all-gather.9.cloned.1.call-update) | async-done | bytes 2097168 | tf_op jit(solution)/shard_map/all_gather | solution.py:36
  89.0 3.0 fusion.9
  92.4 39.0 %all-gather.11.cloned.1.call-done = bf16[2048,512]{1,0:T(8,128)(2,1)} async-done(((bf16[128,512]{1,0:T(8,128)(2,1)}), bf16[2048,512]{1,0:T(8,128)(2,1)}) %all-gather.11.cloned.1.call-update) | async-done | bytes 2097168 | tf_op jit(solution)/shard_map/all_gather | solution.py:58
  131.4 3.9 fusion.2
  135.4 25.0 %reduce-scatter.3.cloned.1.call-done = bf16[1024,384]{0,1:T(8,128)(2,1)} async-done(((bf16[2048,384]{0,1:T(8,128)(2,1)}), bf16[1024,384]{0,1:T(8,128)(2,1)}) %reduce-scatter.3.cloned.1.call-update) | async-done | bytes 786448 | tf_op jit(solution)/shard_map/reduce_scatter | solution.py:59
  160.4 1.7 fusion.11
  162.0 4.9 all-reduce.5
  167.0 1.3 multiply_convert_fusion.2
  168.3 0.5 all-gather.15.cloned.1.call-update
  168.9 0.7 all-gather.17.cloned.1.call-update
  169.7 26.0 %all-gather.13.cloned.1.call-done = bf16[384,2048]{1,0:T(8,128)(2,1)} async-done(((bf16[384,1024]{1,0:T(8,128)(2,1)}), bf16[384,2048]{1,0:T(8,128)(2,1)}) %all-gather.13.cloned.1.call-update) | async-done | bytes 1572880 | tf_op jit(solution)/shard_map/all_gather | solution.py:67
  195.6 128.5 %all-gather.15.cloned.1.call-done = bf16[2048,4096]{1,0:T(8,128)(2,1)} async-done(((bf16[128,4096]{1,0:T(8,128)(2,1)}), bf16[2048,4096]{1,0:T(8,128)(2,1)}) %all-gather.15.cloned.1.call-update) | async-done | bytes 16777232 | tf_op jit(solution)/shard_map/all_gather | solution.py:66
  324.1 126.8 %all-gather.17.cloned.1.call-done = bf16[2048,4096]{1,0:T(8,128)(2,1)} async-done(((bf16[128,4096]{1,0:T(8,128)(2,1)}), bf16[2048,4096]{1,0:T(8,128)(2,1)}) %all-gather.17.cloned.1.call-update) | async-done | bytes 16777232 | tf_op jit(solution)/shard_map/all_gather | solution.py:69
  450.9 19.0 %fusion.3 = bf16[2048,384]{0,1:T(8,128)(2,1)} fusion(bf16[2048,4096]{1,0:T(8,128)(2,1)} %all-gather.17.cloned.1.call-done, bf16[384,2048]{1,0:T(8,128)(2,1)} %all-gather.13.cloned.1.call-done, bf16[2048,4096]{1,0:T(8,128)(2,1)} %all-gather.15.cloned.1.call-done), kind=kOutput, calls=%fused_computation.9 | convolution fusion | flops 12890406912 | bytes 36700160 | tf_op jit(solution)/shard_map/dot_general | solution.py:23
  470.0 24.5 %reduce-scatter.5.cloned.1.call-done = bf16[1024,384]{0,1:T(8,128)(2,1)} async-done(((bf16[2048,384]{0,1:T(8,128)(2,1)}), bf16[1024,384]{0,1:T(8,128)(2,1)}) %reduce-scatter.5.cloned.1.call-update) | async-done | bytes 786448 | tf_op jit(solution)/shard_map/reduce_scatter | solution.py:70
  494.4 1.7 fusion.10
  496.1 4.9 all-reduce.4
  501.1 1.3 multiply_convert_fusion.1
  (36 shorter events, 0.8 us)
Async XLA Ops:
  6.5 38.8 %all-gather.7.cloned.1.call-start = ((), (), s32[]{:S(2)}) async-start(), calls=%async_computation.2 | async-start | bytes 2359296 | tf_op jit(solution)/shard_map/all_gather | solution.py:38
  16.2 72.8 %all-gather.9.cloned.1.call-start = ((), (), s32[]{:S(2)}) async-start(), calls=%async_computation.3 | async-start | bytes 2228224 | tf_op jit(solution)/shard_map/all_gather | solution.py:36
  17.0 114.4 %all-gather.11.cloned.1.call-start = ((), (), s32[]{:S(2)}) async-start(), calls=%async_computation.4 | async-start | bytes 2228224 | tf_op jit(solution)/shard_map/all_gather | solution.py:58
  17.7 142.7 %reduce-scatter.3.cloned.1.call-start = ((), (), s32[]{:S(2)}) async-start(), calls=%async_computation.5 | async-start | bytes 2359296 | tf_op jit(solution)/shard_map/reduce_scatter | solution.py:59
  92.2 39.2 %copy-start.6 = (f32[512]{0:T(512)S(1)}, f32[512]{0:T(512)}, u32[]{:S(2)}) copy-start(f32[512]{0:T(512)} %param.12) | copy-start | bytes 6148
  135.3 25.0 %copy-start = (bf16[384,1024]{1,0:T(8,128)(2,1)S(1)}, bf16[384,1024]{1,0:T(8,128)(2,1)}, u32[]{:S(2)}) copy-start(bf16[384,1024]{1,0:T(8,128)(2,1)} %param.9) | copy-start | bytes 2359300
  135.3 31.6 %copy-start.4 = (f32[1024]{0:T(1024)S(1)}, f32[1024]{0:T(1024)}, u32[]{:S(2)}) copy-start(f32[1024]{0:T(1024)} %param.14) | copy-start | bytes 12292
  135.3 60.3 %all-gather.13.cloned.1.call-start = ((), (), s32[]{:S(2)}) async-start(), calls=%async_computation.6 | async-start | bytes 2359296 | tf_op jit(solution)/shard_map/all_gather | solution.py:67
  160.3 6.6 %copy-start.2 = (bf16[1024,384]{0,1:T(8,128)(2,1)S(1)}, bf16[1024,384]{0,1:T(8,128)(2,1)}, u32[]{:S(2)}) copy-start(bf16[1024,384]{0,1:T(8,128)(2,1)} %reduce-scatter.3.cloned.1.call-done) | copy-start | bytes 2359300
  168.3 155.8 %all-gather.15.cloned.1.call-start = ((), (), s32[]{:S(2)}) async-start(), calls=%async_computation.7 | async-start | bytes 17825792 | tf_op jit(solution)/shard_map/all_gather | solution.py:66
  168.9 282.1 %all-gather.17.cloned.1.call-start = ((), (), s32[]{:S(2)}) async-start(), calls=%async_computation.8 | async-start | bytes 17825792 | tf_op jit(solution)/shard_map/all_gather | solution.py:69
  169.6 324.8 %reduce-scatter.5.cloned.1.call-start = ((), (), s32[]{:S(2)}) async-start(), calls=%async_computation.9 | async-start | bytes 2359296 | tf_op jit(solution)/shard_map/reduce_scatter | solution.py:70
  469.9 24.5 %copy-start.1 = (bf16[384,1024]{1,0:T(8,128)(2,1)S(1)}, bf16[384,1024]{1,0:T(8,128)(2,1)}, u32[]{:S(2)}) copy-start(bf16[384,1024]{1,0:T(8,128)(2,1)} %multiply_convert_fusion.2) | copy-start | bytes 2359300
  469.9 31.1 %copy-start.5 = (f32[1024]{0:T(1024)S(1)}, f32[1024]{0:T(1024)}, u32[]{:S(2)}) copy-start(f32[1024]{0:T(1024)} %param.17) | copy-start | bytes 12292
  494.4 6.6 %copy-start.3 = (bf16[1024,384]{0,1:T(8,128)(2,1)S(1)}, bf16[1024,384]{0,1:T(8,128)(2,1)}, u32[]{:S(2)}) copy-start(bf16[1024,384]{0,1:T(8,128)(2,1)} %reduce-scatter.5.cloned.1.call-done) | copy-start | bytes 2359300
Sparse Core Ops, SparseCore 0:
  16.3 28.9 all-gather.6
  47.5 41.4 all-gather.8
  91.2 40.1 all-gather.10
  135.5 24.8 reduce-scatter.2
  168.4 27.1 all-gather.12
  197.7 126.4 all-gather.14
  326.3 124.5 all-gather.16
  470.1 24.3 reduce-scatter.4
where the time goes:
time: 510 us; the launch traced here: 509 us
  waiting for transfers between devices  444 us (87%)
  matrix products  26 us (5%)
  blocking collectives  15.7 us (3%)
  between operations  13.6 us (3%)
  other arithmetic  10 us (2%)
    all_gather x1, waiting for transfers between devices, local(): up_full = lax.all_gather(w_ff1, 'fs', axis=0, tiled=True)  128 us
    all_gather x1, waiting for transfers between devices, local(): down_full = lax.all_gather(w_ff2, 'fs', axis=0, tiled=True)  127 us
    all_gather x1, waiting for transfers between devices, local(): in_full = lax.all_gather(w_in, 'fs', axis=0, tiled=True)  43.7 us
    all_gather x1, waiting for transfers between devices, local(): out_full = lax.all_gather(w_pool_out, 'fs', axis=0, tiled=True)  39 us
    all_gather x1, waiting for transfers between devices, local(): lax.all_gather(mixed_in, 'tp', axis=1, tiled=True)  27.5 us
    all_gather x1, waiting for transfers between devices, local(): lax.all_gather(middle, 'tp', axis=1, tiled=True)  26 us
    reduce_scatter x1, waiting for transfers between devices, local(): lax.psum_scatter(project_rows(out_full, pooled).astype(jnp.bfloat16), 'tp...  25 us
    reduce_scatter x1, waiting for transfers between devices, local(): lax.psum_scatter(project_rows(down_full, hidden).astype(jnp.bfloat16), 't...  24.5 us
  transfers between devices with their start and end apart: 8, of which 8 were waited for; matrix products, arithmetic and copies ran while one was open for 1% of the time, Pallas kernels for 0%

commit v1 on v0

--- a/solution.py
+++ b/solution.py
@@ -5,6 +5,12 @@
 
 norm_eps = 1e-05
 residual_alpha = 2.0**0.25
+
+
+def all_parts(x, mesh_axis, dim):
+    parts = lax.all_gather(x, mesh_axis, axis=0, tiled=False)
+    whole = jnp.concatenate(parts, axis=dim)
+    return whole
 
 
 def row_norm(value, gain):
@@ -35,7 +41,7 @@
     mixed_in = row_norm(xf, gain_mixer).astype(jnp.bfloat16)
     in_full = lax.all_gather(w_in, "fs", axis=0, tiled=True)
     channels = w_in.shape[1]
-    pool_in = fold_features(in_full, lax.all_gather(mixed_in, "tp", axis=1, tiled=True))
+    pool_in = fold_features(in_full, all_parts(mixed_in, "tp", 1))
     uf = pool_in.astype(jnp.bfloat16).astype(jnp.float32)
     group_width = channels * lax.axis_size("tp") // 4
     channel = lax.axis_index("tp") * channels + jnp.arange(channels, dtype=jnp.int32)

time: 510 us -> 510 us (level)
  no operation moved by 1% of the time
where the time goes in v1:
time: 510 us; the launch traced here: 509 us
  waiting for transfers between devices  442 us (87%)
  matrix products  25.5 us (5%)
  blocking collectives  15.7 us (3%)
  between operations  13.6 us (3%)
  other arithmetic  10 us (2%)
    all_gather x1, waiting for transfers between devices, local(): up_full = lax.all_gather(w_ff1, 'fs', axis=0, tiled=True)  128 us
    all_gather x1, waiting for transfers between devices, local(): down_full = lax.all_gather(w_ff2, 'fs', axis=0, tiled=True)  127 us
    all_gather x1, waiting for transfers between devices, local(): in_full = lax.all_gather(w_in, 'fs', axis=0, tiled=True)  41.8 us
    all_gather x1, waiting for transfers between devices, local(): out_full = lax.all_gather(w_pool_out, 'fs', axis=0, tiled=True)  39.4 us
    all_gather x1, waiting for transfers between devices, all_parts(): parts = lax.all_gather(x, mesh_axis, axis=0, tiled=False)  27.5 us
    all_gather x1, waiting for transfers between devices, local(): lax.all_gather(middle, 'tp', axis=1, tiled=True)  26 us
    reduce_scatter x1, waiting for transfers between devices, local(): lax.psum_scatter(project_rows(out_full, pooled).astype(jnp.bfloat16), 'tp...  25 us
    reduce_scatter x1, waiting for transfers between devices, local(): lax.psum_scatter(project_rows(down_full, hidden).astype(jnp.bfloat16), 't...  24.5 us
  transfers between devices with their start and end apart: 8, of which 8 were waited for; matrix products, arithmetic and copies ran while one was open for 1% of the time, Pallas kernels for 0%

profile of v1, /device:TPU:0, one launch (start us, length us, event | category | flops | bytes accessed | tf_op | source)
XLA Modules:
  0.0 509.2 jit_solution(2970050344120722175)
XLA Ops:
  6.5 1.4 convert_reduce_fusion
  8.0 5.9 %all-reduce.6 = (f32[384]{0:T(512)S(1)}, f32[384]{0:T(512)S(1)}) all-reduce(f32[384]{0:T(512)S(1)} %get-tuple-element.10, f32[384]{0:T(512)S(1)} %get-tuple-element.9), channel_id=1, replica_groups=mesh['fs'=16,'tp'=2] {'tp'}, use_global_device_ids=true, to_apply=%region_3.0 | all-reduce | flops 768 | bytes 6144 | tf_op jit(solution)/shard_map/psum | solution.py:18
  13.9 2.3 fusion.7
  16.3 0.7 all-gather.8.cloned.1.call-update
  17.0 0.7 all-gather.10.cloned.1.call-update
  17.8 27.5 %all-gather.18.cloned.1.call-done = bf16[768,1024]{1,0:T(8,128)(2,1)} async-done(((bf16[384,1024]{1,0:T(8,128)(2,1)}), bf16[768,1024]{1,0:T(8,128)(2,1)}) %all-gather.18.cloned.1.call-update) | async-done | bytes 1572880 | tf_op jit(solution)/shard_map/all_gather | solution.py:11
  45.3 1.9 copy.10
  47.2 41.8 %all-gather.8.cloned.1.call-done = bf16[2048,512]{1,0:T(8,128)(2,1)} async-done(((bf16[128,512]{1,0:T(8,128)(2,1)}), bf16[2048,512]{1,0:T(8,128)(2,1)}) %all-gather.8.cloned.1.call-update) | async-done | bytes 2097168 | tf_op jit(solution)/shard_map/all_gather | solution.py:42
  89.0 2.6 fusion.9
  91.9 39.4 %all-gather.10.cloned.1.call-done = bf16[2048,512]{1,0:T(8,128)(2,1)} async-done(((bf16[128,512]{1,0:T(8,128)(2,1)}), bf16[2048,512]{1,0:T(8,128)(2,1)}) %all-gather.10.cloned.1.call-update) | async-done | bytes 2097168 | tf_op jit(solution)/shard_map/all_gather | solution.py:64
  131.4 3.9 fusion.2
  135.4 25.0 %reduce-scatter.3.cloned.1.call-done = bf16[1024,384]{0,1:T(8,128)(2,1)} async-done(((bf16[2048,384]{0,1:T(8,128)(2,1)}), bf16[1024,384]{0,1:T(8,128)(2,1)}) %reduce-scatter.3.cloned.1.call-update) | async-done | bytes 786448 | tf_op jit(solution)/shard_map/reduce_scatter | solution.py:65
  160.4 1.7 fusion.11
  162.0 4.9 all-reduce.5
  167.0 1.3 multiply_convert_fusion.2
  168.9 0.7 all-gather.16.cloned.1.call-update
  169.7 26.0 %all-gather.12.cloned.1.call-done = bf16[384,2048]{1,0:T(8,128)(2,1)} async-done(((bf16[384,1024]{1,0:T(8,128)(2,1)}), bf16[384,2048]{1,0:T(8,128)(2,1)}) %all-gather.12.cloned.1.call-update) | async-done | bytes 1572880 | tf_op jit(solution)/shard_map/all_gather | solution.py:73
  195.7 128.5 %all-gather.14.cloned.1.call-done = bf16[2048,4096]{1,0:T(8,128)(2,1)} async-done(((bf16[128,4096]{1,0:T(8,128)(2,1)}), bf16[2048,4096]{1,0:T(8,128)(2,1)}) %all-gather.14.cloned.1.call-update) | async-done | bytes 16777232 | tf_op jit(solution)/shard_map/all_gather | solution.py:72
  324.1 126.8 %all-gather.16.cloned.1.call-done = bf16[2048,4096]{1,0:T(8,128)(2,1)} async-done(((bf16[128,4096]{1,0:T(8,128)(2,1)}), bf16[2048,4096]{1,0:T(8,128)(2,1)}) %all-gather.16.cloned.1.call-update) | async-done | bytes 16777232 | tf_op jit(solution)/shard_map/all_gather | solution.py:75
  450.9 19.0 %fusion.3 = bf16[2048,384]{0,1:T(8,128)(2,1)} fusion(bf16[2048,4096]{1,0:T(8,128)(2,1)} %all-gather.16.cloned.1.call-done, bf16[384,2048]{1,0:T(8,128)(2,1)} %all-gather.12.cloned.1.call-done, bf16[2048,4096]{1,0:T(8,128)(2,1)} %all-gather.14.cloned.1.call-done), kind=kOutput, calls=%fused_computation.9 | convolution fusion | flops 12890406912 | bytes 36700160 | tf_op jit(solution)/shard_map/dot_general | solution.py:29
  470.0 24.5 %reduce-scatter.5.cloned.1.call-done = bf16[1024,384]{0,1:T(8,128)(2,1)} async-done(((bf16[2048,384]{0,1:T(8,128)(2,1)}), bf16[1024,384]{0,1:T(8,128)(2,1)}) %reduce-scatter.5.cloned.1.call-update) | async-done | bytes 786448 | tf_op jit(solution)/shard_map/reduce_scatter | solution.py:76
  494.5 1.7 fusion.10
  496.1 4.9 all-reduce.4
  501.1 1.3 multiply_convert_fusion.1
  (37 shorter events, 1.3 us)
Async XLA Ops:
  6.5 38.8 %all-gather.18.cloned.1.call-start = ((), (), s32[]{:S(2)}) async-start(), calls=%async_computation.9 | async-start | bytes 2359296 | tf_op jit(solution)/shard_map/all_gather | solution.py:11
  16.2 72.8 %all-gather.8.cloned.1.call-start = ((), (), s32[]{:S(2)}) async-start(), calls=%async_computation.2 | async-start | bytes 2228224 | tf_op jit(solution)/shard_map/all_gather | solution.py:42
  17.0 114.4 %all-gather.10.cloned.1.call-start = ((), (), s32[]{:S(2)}) async-start(), calls=%async_computation.3 | async-start | bytes 2228224 | tf_op jit(solution)/shard_map/all_gather | solution.py:64
  17.7 142.7 %reduce-scatter.3.cloned.1.call-start = ((), (), s32[]{:S(2)}) async-start(), calls=%async_computation.4 | async-start | bytes 2359296 | tf_op jit(solution)/shard_map/reduce_scatter | solution.py:65
  91.7 39.7 %copy-start.6 = (f32[512]{0:T(512)S(1)}, f32[512]{0:T(512)}, u32[]{:S(2)}) copy-start(f32[512]{0:T(512)} %param.12) | copy-start | bytes 6148
  135.3 25.0 %copy-start = (bf16[384,1024]{1,0:T(8,128)(2,1)S(1)}, bf16[384,1024]{1,0:T(8,128)(2,1)}, u32[]{:S(2)}) copy-start(bf16[384,1024]{1,0:T(8,128)(2,1)} %param.9) | copy-start | bytes 2359300
  135.3 31.6 %copy-start.4 = (f32[1024]{0:T(1024)S(1)}, f32[1024]{0:T(1024)}, u32[]{:S(2)}) copy-start(f32[1024]{0:T(1024)} %param.14) | copy-start | bytes 12292
  135.3 60.3 %all-gather.12.cloned.1.call-start = ((), (), s32[]{:S(2)}) async-start(), calls=%async_computation.5 | async-start | bytes 2359296 | tf_op jit(solution)/shard_map/all_gather | solution.py:73
  160.4 6.6 %copy-start.2 = (bf16[1024,384]{0,1:T(8,128)(2,1)S(1)}, bf16[1024,384]{0,1:T(8,128)(2,1)}, u32[]{:S(2)}) copy-start(bf16[1024,384]{0,1:T(8,128)(2,1)} %reduce-scatter.3.cloned.1.call-done) | copy-start | bytes 2359300
  168.3 155.8 %all-gather.14.cloned.1.call-start = ((), (), s32[]{:S(2)}) async-start(), calls=%async_computation.6 | async-start | bytes 17825792 | tf_op jit(solution)/shard_map/all_gather | solution.py:72
  168.9 282.1 %all-gather.16.cloned.1.call-start = ((), (), s32[]{:S(2)}) async-start(), calls=%async_computation.7 | async-start | bytes 17825792 | tf_op jit(solution)/shard_map/all_gather | solution.py:75
  169.6 324.8 %reduce-scatter.5.cloned.1.call-start = ((), (), s32[]{:S(2)}) async-start(), calls=%async_computation.8 | async-start | bytes 2359296 | tf_op jit(solution)/shard_map/reduce_scatter | solution.py:76
  469.9 24.5 %copy-start.1 = (bf16[384,1024]{1,0:T(8,128)(2,1)S(1)}, bf16[384,1024]{1,0:T(8,128)(2,1)}, u32[]{:S(2)}) copy-start(bf16[384,1024]{1,0:T(8,128)(2,1)} %multiply_convert_fusion.2) | copy-start | bytes 2359300
  469.9 31.1 %copy-start.5 = (f32[1024]{0:T(1024)S(1)}, f32[1024]{0:T(1024)}, u32[]{:S(2)}) copy-start(f32[1024]{0:T(1024)} %param.17) | copy-start | bytes 12292
  494.5 6.6 %copy-start.3 = (bf16[1024,384]{0,1:T(8,128)(2,1)S(1)}, bf16[1024,384]{0,1:T(8,128)(2,1)}, u32[]{:S(2)}) copy-start(bf16[1024,384]{0,1:T(8,128)(2,1)} %reduce-scatter.5.cloned.1.call-done) | copy-start | bytes 2359300
Sparse Core Ops, SparseCore 0:
  16.3 28.9 all-gather.17
  47.5 41.4 all-gather.7
  91.2 40.1 all-gather.9
  135.5 24.8 reduce-scatter.2
  168.4 27.1 all-gather.11
  197.7 126.4 all-gather.13
  326.3 124.5 all-gather.15
  470.1 24.3 reduce-scatter.4
